TPU v7x, 32 devices: a whole 2x2x4 slice. The times are simulated.
32 devices in a mesh: fs: 8 (over z, y), tp: 4 (over x, core).
Axes of the slice: x: 2, y: 2, z: 4, core: 2. Of those that a mesh axis runs over, the one named last changes fastest.
Arguments:
- tokens: bfloat16 [640, 3072], P('tp'), may hold values from -6 to 6
- gain_first: float32 [3072], replicated, may hold values from 0.1 to 1.9
- gain_second: float32 [3072], replicated, may hold values from 0.1 to 1.9
- gate_first: float32 [3072, 8192], P('fs', 'tp'), may hold values from -0.109375 to 0.109375
- up_first: float32 [3072, 8192], P('fs', 'tp'), may hold values from -0.109375 to 0.109375
- down_first: float32 [8192, 3072], P('fs', 'tp'), may hold values from -0.09375 to 0.09375
- gate_second: float32 [3072, 8192], P('fs', 'tp'), may hold values from -0.109375 to 0.109375
- up_second: float32 [3072, 8192], P('fs', 'tp'), may hold values from -0.109375 to 0.109375
- down_second: float32 [8192, 3072], P('fs', 'tp'), may hold values from -0.09375 to 0.09375
Outputs:
- result_rows: bfloat16 [640, 3072], P('tp')
- serve_gate_first: bfloat16 [3072, 8192], P(None, 'fs')
- serve_up_first: bfloat16 [3072, 8192], P(None, 'fs')
- serve_down_first: bfloat16 [8192, 3072], P('fs')
- serve_gate_second: bfloat16 [3072, 8192], P(None, 'fs')
- serve_up_second: bfloat16 [3072, 8192], P(None, 'fs')
- serve_down_second: bfloat16 [8192, 3072], P('fs')
All inputs are finite; a program needn't handle non-finite values.
Results may differ from a plain program's by a relative error of at most 0.011.
Values may be sent and summed in bfloat16 or wider, within the bound.
A program may use at most 192 MiB of HBM per device.

v0:
```python
import jax
import jax.numpy as jnp
from jax import lax
from jax.sharding import PartitionSpec as P


def plain_norm(values):
    values = values.astype(jnp.float32)
    center = jnp.mean(values, axis=-1, keepdims=True)
    spread = jnp.mean(jnp.square(values - center), axis=-1, keepdims=True)
    return (values - center) * lax.rsqrt(spread + 1e-05)


def sum_over_hidden(partial_value):
    pieces = lax.all_to_all(
        partial_value.astype(jnp.bfloat16), "fs", split_axis=1, concat_axis=0, tiled=True
    )
    rows = partial_value.shape[0]
    pieces = pieces.reshape(-1, rows, pieces.shape[1]).astype(jnp.float32)
    summed = jnp.sum(pieces, axis=0).astype(jnp.bfloat16)
    return lax.all_gather(summed, "fs", axis=1, tiled=True).astype(jnp.float32)


def regroup(folded):
    spread = lax.all_to_all(folded, "tp", split_axis=0, concat_axis=1, tiled=True)
    parts = lax.axis_size("fs")
    rows = spread.shape[0]
    owned = lax.all_to_all(spread, "fs", split_axis=1, concat_axis=0, tiled=True)
    owned = owned.reshape(parts, rows, owned.shape[1])
    whole = lax.all_gather(owned, "tp", axis=1, tiled=True)
    return whole.reshape(-1, whole.shape[2])


def half_step(normed, scales, w_gate, w_rising, w_down):
    gate_part = jnp.dot(normed, w_gate, preferred_element_type=jnp.float32)
    rising = jnp.dot(normed, w_rising, preferred_element_type=jnp.float32)
    hidden = (jax.nn.silu(gate_part) * rising).astype(jnp.bfloat16)
    partial_value = jnp.dot(hidden, w_down, preferred_element_type=jnp.float32)
    block = sum_over_hidden(partial_value)
    mixed = 1.6817928 * scales[None, :] * normed.astype(jnp.float32) + 0.5 * block
    return plain_norm(mixed).astype(jnp.bfloat16)


def on_device(
    tokens,
    gain_first,
    gain_second,
    gate_first,
    up_first,
    down_first,
    gate_second,
    up_second,
    down_second,
):
    row_count = gate_first.shape[0]
    offset = lax.axis_index("fs") * row_count

    def fold_gain(weight, scales):
        picked = lax.dynamic_slice_in_dim(scales, offset, row_count, 0)
        return (picked[:, None] * weight).astype(jnp.bfloat16)

    serve_gate_first = regroup(fold_gain(gate_first, gain_first))
    serve_up_first = regroup(fold_gain(up_first, gain_first))
    serve_down_first = lax.all_gather(down_first.astype(jnp.bfloat16), "tp", axis=1, tiled=True)
    serve_gate_second = regroup(fold_gain(gate_second, gain_second))
    serve_up_second = regroup(fold_gain(up_second, gain_second))
    serve_down_second = lax.all_gather(down_second.astype(jnp.bfloat16), "tp", axis=1, tiled=True)
    normed_zero = plain_norm(tokens).astype(jnp.bfloat16)
    normed_one = half_step(
        normed_zero, gain_first, serve_gate_first, serve_up_first, serve_down_first
    )
    result_rows = half_step(
        normed_one, gain_second, serve_gate_second, serve_up_second, serve_down_second
    )
    return (
        result_rows,
        serve_gate_first,
        serve_up_first,
        serve_down_first,
        serve_gate_second,
        serve_up_second,
        serve_down_second,
    )


def solution(mesh):
    placed = (
        P("tp", None),
        P(),
        P(),
        P("fs", "tp"),
        P("fs", "tp"),
        P("fs", "tp"),
        P("fs", "tp"),
        P("fs", "tp"),
        P("fs", "tp"),
    )
    return jax.shard_map(
        on_device,
        mesh=mesh,
        in_specs=placed,
        out_specs=(
            P("tp", None),
            P(None, "fs"),
            P(None, "fs"),
            P("fs", None),
            P(None, "fs"),
            P(None, "fs"),
            P("fs", None),
        ),
        check_vma=False,
    )
```

profile of v0, /device:TPU:0, one launch (start us, length us, event | category | flops | bytes accessed | tf_op | source)
XLA Modules:
  0.0 523.0 jit_solution(2696292961990616382)
XLA Ops:
  8.0 3.7 multiply_convert_fusion.3
  11.7 24.1 %all_to_all.154 = bf16[4,96,2048]{2,1,0:T(8,128)(2,1)S(1)} all-to-all(bf16[4,96,2048]{2,1,0:T(8,128)(2,1)S(1)} %bitcast.44), channel_id=1, replica_groups=mesh['fs'=8,'tp'=4] {'tp'}, dimensions={0} | all-to-all | bytes 3145728 | tf_op jit(solution)/shard_map/all_to_all | solution.py:25
  37.0 1.8 all_to_all.119
  38.9 2.3 copy.29
  41.2 42.3 %all_to_all.155 = bf16[96,8,1024]{2,0,1:T(8,128)(2,1)S(1)} all-to-all(bf16[96,8,1024]{2,0,1:T(8,128)(2,1)S(1)} %copy.29), channel_id=1, replica_groups=mesh['fs'=8,'tp'=4] {'fs'}, dimensions={1} | all-to-all | bytes 3145728 | tf_op jit(solution)/shard_map/all_to_all | solution.py:28
  83.5 2.0 copy.30
  85.6 36.1 %all_to_all.156 = bf16[4,96,2048]{2,1,0:T(8,128)(2,1)S(1)} all-to-all(bf16[4,96,2048]{2,1,0:T(8,128)(2,1)S(1)} %bitcast.42), channel_id=1, replica_groups=mesh['fs'=8,'tp'=4] {'tp'}, dimensions={0} | all-to-all | bytes 3145728 | tf_op jit(solution)/shard_map/all_to_all | solution.py:25
  124.2 39.1 %all_to_all.157 = bf16[96,8,1024]{2,0,1:T(8,128)(2,1)S(1)} all-to-all(bf16[96,8,1024]{2,0,1:T(8,128)(2,1)S(1)} %copy.33), channel_id=1, replica_groups=mesh['fs'=8,'tp'=4] {'fs'}, dimensions={1} | all-to-all | bytes 3145728 | tf_op jit(solution)/shard_map/all_to_all | solution.py:28
  163.3 2.0 copy.34
  166.8 3.9 multiply_convert_fusion.1
  170.7 39.8 %all_to_all.158 = bf16[4,96,2048]{2,1,0:T(8,128)(2,1)S(1)} all-to-all(bf16[4,96,2048]{2,1,0:T(8,128)(2,1)S(1)} %bitcast.45), channel_id=1, replica_groups=mesh['fs'=8,'tp'=4] {'tp'}, dimensions={0} | all-to-all | bytes 3145728 | tf_op jit(solution)/shard_map/all_to_all | solution.py:25
  211.7 1.8 all_to_all.133
  213.6 2.3 copy.38
  215.8 51.1 %all_to_all.159 = bf16[96,8,1024]{2,0,1:T(8,128)(2,1)S(1)} all-to-all(bf16[96,8,1024]{2,0,1:T(8,128)(2,1)S(1)} %copy.38), channel_id=1, replica_groups=mesh['fs'=8,'tp'=4] {'fs'}, dimensions={1} | all-to-all | bytes 3145728 | tf_op jit(solution)/shard_map/all_to_all | solution.py:28
  266.9 2.0 copy.39
  269.0 26.1 %all_to_all.160 = bf16[4,96,2048]{2,1,0:T(8,128)(2,1)S(1)} all-to-all(bf16[4,96,2048]{2,1,0:T(8,128)(2,1)S(1)} %bitcast.43), channel_id=1, replica_groups=mesh['fs'=8,'tp'=4] {'tp'}, dimensions={0} | all-to-all | bytes 3145728 | tf_op jit(solution)/shard_map/all_to_all | solution.py:25
  297.6 39.2 %all_to_all.161 = bf16[96,8,1024]{2,0,1:T(8,128)(2,1)S(1)} all-to-all(bf16[96,8,1024]{2,0,1:T(8,128)(2,1)S(1)} %copy.42), channel_id=1, replica_groups=mesh['fs'=8,'tp'=4] {'fs'}, dimensions={1} | all-to-all | bytes 3145728 | tf_op jit(solution)/shard_map/all_to_all | solution.py:28
  336.8 2.0 copy.43
  342.0 9.7 %copy.31 = bf16[8,384,1024]{2,1,0:T(8,128)(2,1)} copy(bf16[8,384,1024]{2,0,1:T(8,128)(2,1)} %all-gather.7.cloned.1.call-done) | data formatting | bytes 12582912 | tf_op jit(solution)/shard_map/all_gather | solution.py:30
  351.7 9.2 %copy.35 = bf16[8,384,1024]{2,1,0:T(8,128)(2,1)} copy(bf16[8,384,1024]{2,0,1:T(8,128)(2,1)} %all-gather.9.cloned.1.call-done) | data formatting | bytes 12582912 | tf_op jit(solution)/shard_map/all_gather | solution.py:30
  362.3 7.0 %convolution_convert_fusion.1 = bf16[160,3072]{1,0:T(8,128)(2,1)S(1)} fusion(bf16[1024,3072]{1,0:T(8,128)(2,1)} %all-gather.11.cloned.1.call-done, bf16[3072,1024]{1,0:T(8,128)(2,1)} %bitcast.38, f32[160,1024]{1,0:T(8,128)S(1)} %fusion.14, bf16[160,3072]{1,0:T(8,128)(2,1)S(1)} %copy-done.1, f32[160]{0:T(256)S(1)} %add_rsqrt_fusion.2, ...), kind=kOutput, calls=%fused_computation.1 | convolution fusion | flops 2016706560 | bytes 15205632 | tf_op jit(solution)/shard_map/dot_general | solution.py:38
  370.3 3.8 all-to-all-start.4
  374.1 9.1 %copy.40 = bf16[8,384,1024]{2,1,0:T(8,128)(2,1)} copy(bf16[8,384,1024]{2,0,1:T(8,128)(2,1)} %all-gather.13.cloned.1.call-done) | data formatting | bytes 12582912 | tf_op jit(solution)/shard_map/all_gather | solution.py:30
  383.7 9.0 %copy.44 = bf16[8,384,1024]{2,1,0:T(8,128)(2,1)} copy(bf16[8,384,1024]{2,0,1:T(8,128)(2,1)} %all-gather.15.cloned.1.call-done) | data formatting | bytes 12582912 | tf_op jit(solution)/shard_map/all_gather | solution.py:30
  392.7 5.5 %all-to-all-done.4 = bf16[160,8,384]{2,0,1:T(8,128)(2,1)S(1)} async-done(((bf16[160,8,384]{2,0,1:T(8,128)(2,1)}), bf16[160,8,384]{2,0,1:T(8,128)(2,1)S(1)}, u32[]{:S(2)}, u32[]{:S(2)}) %all-to-all-start.4) | async-done | bytes 983072 | tf_op jit(solution)/shard_map/all_to_all | solution.py:15
  398.3 33.7 %all_gather.27 = bf16[160,3072]{1,0:T(8,128)(2,1)S(1)} all-gather(bf16[160,384]{1,0:T(8,128)(2,1)S(1)} %reduce_sum.80), channel_id=1, replica_groups=mesh['fs'=8,'tp'=4] {'fs'}, dimensions={1}, use_global_device_ids=true | all-gather | bytes 1105920 | tf_op jit(solution)/shard_map/all_gather | solution.py:21
  436.0 6.9 %convolution_convert_fusion = bf16[160,3072]{1,0:T(8,128)(2,1)S(1)} fusion(bf16[1024,3072]{1,0:T(8,128)(2,1)} %all-gather.17.cloned.1.call-done, bf16[160,3072]{1,0:T(8,128)(2,1)S(1)} %multiply_convert_fusion.5, bf16[3072,1024]{1,0:T(8,128)(2,1)} %bitcast.40, f32[160,1024]{1,0:T(8,128)S(1)} %fusion.16), kind=kOutput, calls=%fused_computation | convolution fusion | flops 2014740480 | bytes 15204352 | tf_op jit(solution)/shard_map/dot_general | solution.py:38
  444.0 3.6 all-to-all-start.9
  447.6 23.0 %all-to-all-done.9 = bf16[160,8,384]{2,0,1:T(8,128)(2,1)S(1)} async-done(((bf16[160,8,384]{2,0,1:T(8,128)(2,1)}), bf16[160,8,384]{2,0,1:T(8,128)(2,1)S(1)}, u32[]{:S(2)}, u32[]{:S(2)}) %all-to-all-start.9) | async-done | bytes 983072 | tf_op jit(solution)/shard_map/all_to_all | solution.py:15
  470.6 33.6 %all_gather.31 = bf16[160,3072]{1,0:T(8,128)(2,1)S(1)} all-gather(bf16[160,384]{1,0:T(8,128)(2,1)S(1)} %reduce_sum.83), channel_id=1, replica_groups=mesh['fs'=8,'tp'=4] {'fs'}, dimensions={1}, use_global_device_ids=true | all-gather | bytes 1105920 | tf_op jit(solution)/shard_map/all_gather | solution.py:21
  506.9 6.1 %copy.54 = bf16[1024,3072]{1,0:T(8,128)(2,1)} copy(bf16[1024,3072]{1,0:T(8,128)(2,1)} %all-gather.11.cloned.1.call-done) | data formatting | bytes 12582912
  513.0 2.7 copy.55
  (71 shorter events, 23.9 us)
Async XLA Ops:
  7.2 334.9 %all-gather.7.cloned.1.call-start = ((), (), s32[]{:S(2)}) async-start(), calls=%async_computation.10 | async-start | bytes 7864320 | tf_op jit(solution)/shard_map/all_gather | solution.py:30
  85.5 266.2 %all-gather.9.cloned.1.call-start = ((), (), s32[]{:S(2)}) async-start(), calls=%async_computation.11 | async-start | bytes 7864320 | tf_op jit(solution)/shard_map/all_gather | solution.py:30
  163.3 2.1 copy-start.3
  165.3 1.4 copy-start.6
  165.3 196.9 %all-gather.11.cloned.1.call-start = ((), (), s32[]{:S(2)}) async-start(), calls=%async_computation.12 | async-start | bytes 7864320 | tf_op jit(solution)/shard_map/all_gather | solution.py:64
  166.7 207.4 %all-gather.13.cloned.1.call-start = ((), (), s32[]{:S(2)}) async-start(), calls=%async_computation.13 | async-start | bytes 7864320 | tf_op jit(solution)/shard_map/all_gather | solution.py:30
  269.0 114.7 %all-gather.15.cloned.1.call-start = ((), (), s32[]{:S(2)}) async-start(), calls=%async_computation.14 | async-start | bytes 7864320 | tf_op jit(solution)/shard_map/all_gather | solution.py:30
  336.8 2.1 copy-start.4
  338.8 97.2 %all-gather.17.cloned.1.call-start = ((), (), s32[]{:S(2)}) async-start(), calls=%async_computation.15 | async-start | bytes 7864320 | tf_op jit(solution)/shard_map/all_gather | solution.py:67
  340.2 1.2 copy-start.1
  351.7 9.2 %copy-start.2 = (bf16[8,384,1024]{2,1,0:T(8,128)(2,1)S(1)}, bf16[8,384,1024]{2,1,0:T(8,128)(2,1)}, u32[]{:S(2)}) copy-start(bf16[8,384,1024]{2,1,0:T(8,128)(2,1)} %copy.31) | copy-start | bytes 18874372
  369.3 4.8 copy-start.5
  370.3 27.8 %all-to-all-start.4 = ((bf16[160,8,384]{2,0,1:T(8,128)(2,1)}), bf16[160,8,384]{2,0,1:T(8,128)(2,1)S(1)}, u32[]{:S(2)}, u32[]{:S(2)}) async-start(bf16[160,8,384]{2,0,1:T(8,128)(2,1)} %bitcast.31), calls=%async_computation.4 | async-start | bytes 1966080 | tf_op jit(solution)/shard_map/all_to_all | solution.py:15
  432.0 2.8 copy-start
  444.0 26.5 %all-to-all-start.9 = ((bf16[160,8,384]{2,0,1:T(8,128)(2,1)}), bf16[160,8,384]{2,0,1:T(8,128)(2,1)S(1)}, u32[]{:S(2)}, u32[]{:S(2)}) async-start(bf16[160,8,384]{2,0,1:T(8,128)(2,1)} %bitcast.30), calls=%async_computation.9 | async-start | bytes 1966080 | tf_op jit(solution)/shard_map/all_to_all | solution.py:15
  505.4 7.6 %slice-start = ((s8[6291456]{0:T(1024)(128)(4,1)}), s8[4194304]{0:T(1024)(128)(4,1)S(1)}, s32[]{:S(2)}) async-start(s8[6291456]{0:T(1024)(128)(4,1)} %bitcast.34), calls=%async_computation.16 | async-start | bytes 8388608
  506.9 6.1 %slice-start.1 = ((s8[6291456]{0:T(1024)(128)(4,1)}), s8[2097152]{0:T(1024)(128)(4,1)S(1)}, s32[]{:S(2)}) async-start(s8[6291456]{0:T(1024)(128)(4,1)} %bitcast.34), calls=%async_computation.17 | async-start | bytes 4194304
Sparse Core Ops, SparseCore 0:
  85.6 57.7 all-gather.6
  165.4 61.2 all-gather.8
  228.8 46.1 all-gather.10
  276.5 50.4 all-gather.12
  338.9 44.6 all-gather.14
  385.7 46.3 all-gather.16
where the time goes:
time: 532 us; the launch traced here: 523 us
  blocking collectives  365 us (69%)
  local copies, waits for them, and re-layouts  74 us (14%)
  waiting for transfers between devices  29.1 us (5%)
  matrix products  16.4 us (3%)
  other arithmetic  16.1 us (3%)
  between operations  14.8 us (3%)
  starting transfers between devices  7.57 us (1%)
    all_to_all x4, blocking collectives, regroup(): lax.all_to_all(spread, 'fs', split_axis=1, concat_axis=0, tiled=True)  172 us
    all_to_all x4, blocking collectives, regroup(): lax.all_to_all(folded, 'tp', split_axis=0, concat_axis=1, tiled=True)  126 us
    all_gather x2, blocking collectives, sum_over_hidden(): return lax.all_gather(summed, 'fs', axis=1, tiled=True).astype(jnp.float32)  67.3 us
    all_gather x4, local copies, waits for them, and re-layouts, regroup(): whole = lax.all_gather(owned, 'tp', axis=1, tiled=True)  36.9 us
    all_to_all x2, waiting for transfers between devices, sum_over_hidden(): lax.all_to_all(partial_value.astype(jnp.bfloat16), 'fs', split_axis=1, co...  28.4 us
    all_to_all x12, local copies, waits for them, and re-layouts, regroup(): lax.all_to_all(spread, 'fs', split_axis=1, concat_axis=0, tiled=True)  18.8 us
    dot_general x2, matrix products, half_step(): partial_value = jnp.dot(hidden, w_down, preferred_element_type=jnp.float32)  13.9 us
  transfers between devices with their start and end apart: 8, of which 3 were waited for; matrix products, arithmetic and copies ran while one was open for 14% of the time, Pallas kernels for 0%

commit v1 on v0

--- a/solution.py
+++ b/solution.py
@@ -18,7 +18,7 @@
     rows = partial_value.shape[0]
     pieces = pieces.reshape(-1, rows, pieces.shape[1]).astype(jnp.float32)
     summed = jnp.sum(pieces, axis=0).astype(jnp.bfloat16)
-    return lax.all_gather(summed, "fs", axis=1, tiled=True).astype(jnp.float32)
+    return jnp.concatenate(lax.all_gather(summed, "fs"), axis=1).astype(jnp.float32)
 
 
 def regroup(folded):

time: 532 us -> 529 us (level)
    all_to_all x4, blocking collectives: 172 us -> 164 us  [regroup(): lax.all_to_all(spread, 'fs', split_axis=1, concat_axis=0, tiled=True)]
    all_to_all x4, blocking collectives: 126 us -> 132 us  [regroup(): lax.all_to_all(folded, 'tp', split_axis=0, concat_axis=1, tiled=True)]
where the time goes in v1:
time: 529 us; the launch traced here: 520 us
  blocking collectives  362 us (68%)
  local copies, waits for them, and re-layouts  73.3 us (14%)
  waiting for transfers between devices  30.2 us (6%)
  matrix products  16.5 us (3%)
  other arithmetic  15.7 us (3%)
  between operations  14.7 us (3%)
  starting transfers between devices  7.89 us (1%)
    all_to_all x4, blocking collectives, regroup(): lax.all_to_all(spread, 'fs', split_axis=1, concat_axis=0, tiled=True)  164 us
    all_to_all x4, blocking collectives, regroup(): lax.all_to_all(folded, 'tp', split_axis=0, concat_axis=1, tiled=True)  132 us
    all_gather x2, blocking collectives, sum_over_hidden(): lax.all_gather(summed, 'fs')  65.9 us
    all_gather x4, local copies, waits for them, and re-layouts, regroup(): whole = lax.all_gather(owned, 'tp', axis=1, tiled=True)  36.6 us
    all_to_all x2, waiting for transfers between devices, sum_over_hidden(): lax.all_to_all(partial_value.astype(jnp.bfloat16), 'fs', split_axis=1, co...  28.9 us
    all_to_all x12, local copies, waits for them, and re-layouts, regroup(): lax.all_to_all(spread, 'fs', split_axis=1, concat_axis=0, tiled=True)  18.8 us
    dot_general x2, matrix products, half_step(): partial_value = jnp.dot(hidden, w_down, preferred_element_type=jnp.float32)  14 us
  transfers between devices with their start and end apart: 8, of which 3 were waited for; matrix products, arithmetic and copies ran while one was open for 14% of the time, Pallas kernels for 0%

profile of v1, /device:TPU:0, one launch (start us, length us, event | category | flops | bytes accessed | tf_op | source)
XLA Modules:
  0.0 520.1 jit_solution(5651162563330914459)
XLA Ops:
  8.0 3.7 multiply_convert_fusion.3
  11.7 24.1 %all_to_all.154 = bf16[4,96,2048]{2,1,0:T(8,128)(2,1)S(1)} all-to-all(bf16[4,96,2048]{2,1,0:T(8,128)(2,1)S(1)} %bitcast.66), channel_id=1, replica_groups=mesh['fs'=8,'tp'=4] {'tp'}, dimensions={0} | all-to-all | bytes 3145728 | tf_op jit(solution)/shard_map/all_to_all | solution.py:25
  37.0 1.8 all_to_all.119
  38.9 2.3 copy.31
  41.2 42.3 %all_to_all.155 = bf16[96,8,1024]{2,0,1:T(8,128)(2,1)S(1)} all-to-all(bf16[96,8,1024]{2,0,1:T(8,128)(2,1)S(1)} %copy.31), channel_id=1, replica_groups=mesh['fs'=8,'tp'=4] {'fs'}, dimensions={1} | all-to-all | bytes 3145728 | tf_op jit(solution)/shard_map/all_to_all | solution.py:28
  83.5 2.0 copy.32
  85.6 36.1 %all_to_all.156 = bf16[4,96,2048]{2,1,0:T(8,128)(2,1)S(1)} all-to-all(bf16[4,96,2048]{2,1,0:T(8,128)(2,1)S(1)} %bitcast.64), channel_id=1, replica_groups=mesh['fs'=8,'tp'=4] {'tp'}, dimensions={0} | all-to-all | bytes 3145728 | tf_op jit(solution)/shard_map/all_to_all | solution.py:25
  124.2 39.1 %all_to_all.157 = bf16[96,8,1024]{2,0,1:T(8,128)(2,1)S(1)} all-to-all(bf16[96,8,1024]{2,0,1:T(8,128)(2,1)S(1)} %copy.35), channel_id=1, replica_groups=mesh['fs'=8,'tp'=4] {'fs'}, dimensions={1} | all-to-all | bytes 3145728 | tf_op jit(solution)/shard_map/all_to_all | solution.py:28
  163.3 2.0 copy.36
  166.8 3.9 multiply_convert_fusion.1
  170.7 39.8 %all_to_all.158 = bf16[4,96,2048]{2,1,0:T(8,128)(2,1)S(1)} all-to-all(bf16[4,96,2048]{2,1,0:T(8,128)(2,1)S(1)} %bitcast.67), channel_id=1, replica_groups=mesh['fs'=8,'tp'=4] {'tp'}, dimensions={0} | all-to-all | bytes 3145728 | tf_op jit(solution)/shard_map/all_to_all | solution.py:25
  211.7 1.8 all_to_all.133
  213.6 2.3 copy.41
  215.8 40.1 %all_to_all.159 = bf16[96,8,1024]{2,0,1:T(8,128)(2,1)S(1)} all-to-all(bf16[96,8,1024]{2,0,1:T(8,128)(2,1)S(1)} %copy.41), channel_id=1, replica_groups=mesh['fs'=8,'tp'=4] {'fs'}, dimensions={1} | all-to-all | bytes 3145728 | tf_op jit(solution)/shard_map/all_to_all | solution.py:28
  255.9 2.0 copy.42
  258.0 32.2 %all_to_all.160 = bf16[4,96,2048]{2,1,0:T(8,128)(2,1)S(1)} all-to-all(bf16[4,96,2048]{2,1,0:T(8,128)(2,1)S(1)} %bitcast.65), channel_id=1, replica_groups=mesh['fs'=8,'tp'=4] {'tp'}, dimensions={0} | all-to-all | bytes 3145728 | tf_op jit(solution)/shard_map/all_to_all | solution.py:25
  292.7 42.4 %all_to_all.161 = bf16[96,8,1024]{2,0,1:T(8,128)(2,1)S(1)} all-to-all(bf16[96,8,1024]{2,0,1:T(8,128)(2,1)S(1)} %copy.45), channel_id=1, replica_groups=mesh['fs'=8,'tp'=4] {'fs'}, dimensions={1} | all-to-all | bytes 3145728 | tf_op jit(solution)/shard_map/all_to_all | solution.py:28
  335.1 2.0 copy.46
  340.4 9.4 %copy.33 = bf16[8,384,1024]{2,1,0:T(8,128)(2,1)} copy(bf16[8,384,1024]{2,0,1:T(8,128)(2,1)} %all-gather.9.cloned.1.call-done) | data formatting | bytes 12582912 | tf_op jit(solution)/shard_map/all_gather | solution.py:30
  349.8 9.1 %copy.37 = bf16[8,384,1024]{2,1,0:T(8,128)(2,1)} copy(bf16[8,384,1024]{2,0,1:T(8,128)(2,1)} %all-gather.11.cloned.1.call-done) | data formatting | bytes 12582912 | tf_op jit(solution)/shard_map/all_gather | solution.py:30
  360.2 7.1 %convolution_convert_fusion.1 = bf16[160,3072]{1,0:T(8,128)(2,1)S(1)} fusion(bf16[1024,3072]{1,0:T(8,128)(2,1)} %all-gather.13.cloned.1.call-done, bf16[3072,1024]{1,0:T(8,128)(2,1)} %bitcast.60, f32[160,1024]{1,0:T(8,128)S(1)} %fusion.14, bf16[160,3072]{1,0:T(8,128)(2,1)S(1)} %copy-done, f32[160]{0:T(256)S(1)} %add_rsqrt_fusion.2, ...), kind=kOutput, calls=%fused_computation.1 | convolution fusion | flops 2016706560 | bytes 15205632 | tf_op jit(solution)/shard_map/dot_general | solution.py:38
  368.4 4.1 all-to-all-start.4
  372.5 9.1 %copy.43 = bf16[8,384,1024]{2,1,0:T(8,128)(2,1)} copy(bf16[8,384,1024]{2,0,1:T(8,128)(2,1)} %all-gather.15.cloned.1.call-done) | data formatting | bytes 12582912 | tf_op jit(solution)/shard_map/all_gather | solution.py:30
  382.6 9.0 %copy.47 = bf16[8,384,1024]{2,1,0:T(8,128)(2,1)} copy(bf16[8,384,1024]{2,0,1:T(8,128)(2,1)} %all-gather.17.cloned.1.call-done) | data formatting | bytes 12582912 | tf_op jit(solution)/shard_map/all_gather | solution.py:30
  391.6 5.1 all-to-all-done.4
  396.9 33.0 %all-gather = bf16[1280,384]{1,0:T(8,128)(2,1)S(1)} all-gather(bf16[160,384]{1,0:T(8,128)(2,1)S(1)} %reduce_sum.80), channel_id=2, replica_groups=mesh['fs'=8,'tp'=4] {'fs'}, dimensions={0}, use_global_device_ids=true | all-gather | bytes 1105920 | tf_op jit(solution)/shard_map/all_gather | solution.py:21
  434.1 6.9 %convolution_convert_fusion = bf16[160,3072]{1,0:T(8,128)(2,1)S(1)} fusion(bf16[1024,3072]{1,0:T(8,128)(2,1)} %all-gather.19.cloned.1.call-done, bf16[160,3072]{1,0:T(8,128)(2,1)S(1)} %multiply_convert_fusion.5, bf16[3072,1024]{1,0:T(8,128)(2,1)} %bitcast.62, f32[160,1024]{1,0:T(8,128)S(1)} %fusion.16), kind=kOutput, calls=%fused_computation | convolution fusion | flops 2014740480 | bytes 15204352 | tf_op jit(solution)/shard_map/dot_general | solution.py:38
  442.1 3.6 all-to-all-start.9
  445.7 23.9 %all-to-all-done.9 = bf16[160,8,384]{2,0,1:T(8,128)(2,1)S(1)} async-done(((bf16[160,8,384]{2,0,1:T(8,128)(2,1)}), bf16[160,8,384]{2,0,1:T(8,128)(2,1)S(1)}, u32[]{:S(2)}, u32[]{:S(2)}) %all-to-all-start.9) | async-done | bytes 983072 | tf_op jit(solution)/shard_map/all_to_all | solution.py:15
  469.7 32.9 %all-gather.1 = bf16[1280,384]{1,0:T(8,128)(2,1)S(1)} all-gather(bf16[160,384]{1,0:T(8,128)(2,1)S(1)} %reduce_sum.83), channel_id=3, replica_groups=mesh['fs'=8,'tp'=4] {'fs'}, dimensions={0}, use_global_device_ids=true | all-gather | bytes 1105920 | tf_op jit(solution)/shard_map/all_gather | solution.py:21
  505.7 3.2 copy.60
  510.4 2.7 copy.61
  (83 shorter events, 26.6 us)
Async XLA Ops:
  7.2 333.2 %all-gather.9.cloned.1.call-start = ((), (), s32[]{:S(2)}) async-start(), calls=%async_computation.10 | async-start | bytes 7864320 | tf_op jit(solution)/shard_map/all_gather | solution.py:30
  85.5 264.3 %all-gather.11.cloned.1.call-start = ((), (), s32[]{:S(2)}) async-start(), calls=%async_computation.11 | async-start | bytes 7864320 | tf_op jit(solution)/shard_map/all_gather | solution.py:30
  163.3 2.1 copy-start.2
  165.3 1.4 copy-start.5
  165.3 194.9 %all-gather.13.cloned.1.call-start = ((), (), s32[]{:S(2)}) async-start(), calls=%async_computation.12 | async-start | bytes 7864320 | tf_op jit(solution)/shard_map/all_gather | solution.py:64
  166.7 205.8 %all-gather.15.cloned.1.call-start = ((), (), s32[]{:S(2)}) async-start(), calls=%async_computation.13 | async-start | bytes 7864320 | tf_op jit(solution)/shard_map/all_gather | solution.py:30
  258.0 124.7 %all-gather.17.cloned.1.call-start = ((), (), s32[]{:S(2)}) async-start(), calls=%async_computation.14 | async-start | bytes 7864320 | tf_op jit(solution)/shard_map/all_gather | solution.py:30
  335.1 2.1 copy-start.3
  337.1 97.0 %all-gather.19.cloned.1.call-start = ((), (), s32[]{:S(2)}) async-start(), calls=%async_computation.15 | async-start | bytes 7864320 | tf_op jit(solution)/shard_map/all_gather | solution.py:67
  338.5 1.2 copy-start
  349.8 9.2 %copy-start.1 = (bf16[8,384,1024]{2,1,0:T(8,128)(2,1)S(1)}, bf16[8,384,1024]{2,1,0:T(8,128)(2,1)}, u32[]{:S(2)}) copy-start(bf16[8,384,1024]{2,1,0:T(8,128)(2,1)} %copy.33) | copy-start | bytes 18874372
  367.3 5.1 copy-start.4
  368.4 28.3 %all-to-all-start.4 = ((bf16[160,8,384]{2,0,1:T(8,128)(2,1)}), bf16[160,8,384]{2,0,1:T(8,128)(2,1)S(1)}, u32[]{:S(2)}, u32[]{:S(2)}) async-start(bf16[160,8,384]{2,0,1:T(8,128)(2,1)} %bitcast.41), calls=%async_computation.4 | async-start | bytes 1966080 | tf_op jit(solution)/shard_map/all_to_all | solution.py:15
  429.9 2.4 slice-start
  430.2 2.6 slice-start.1
  442.1 27.4 %all-to-all-start.9 = ((bf16[160,8,384]{2,0,1:T(8,128)(2,1)}), bf16[160,8,384]{2,0,1:T(8,128)(2,1)S(1)}, u32[]{:S(2)}, u32[]{:S(2)}) async-start(bf16[160,8,384]{2,0,1:T(8,128)(2,1)} %bitcast.40), calls=%async_computation.9 | async-start | bytes 1966080 | tf_op jit(solution)/shard_map/all_to_all | solution.py:15
  502.5 2.7 slice-start.2
  502.9 2.9 slice-start.3
  503.8 5.2 slice-start.4
  505.7 4.6 slice-start.5
Sparse Core Ops, SparseCore 0:
  85.6 57.7 all-gather.8
  165.4 61.2 all-gather.10
  228.8 55.9 all-gather.12
  286.2 48.5 all-gather.14
  337.3 45.3 all-gather.16
  384.6 46.3 all-gather.18
